TPU v7x, 32 devices: a whole 2x2x4 slice. The times are simulated.
32 devices in a mesh: grp: 2 (over y), fs: 4 (over z), tp: 4 (over x, core).
Axes of the slice: x: 2, y: 2, z: 4, core: 2. Of those that a mesh axis runs over, the one named last changes fastest.
Arguments:
- tokens: bfloat16 [8, 1024, 2048], P(('grp', 'fs'), None, 'tp'), parts along dimension 0, may hold values from -6 to 6
- mix_gain: float32 [2048], replicated, may hold values from 0.1 to 1.9
- in_matrix: float32 [2048, 1024], P('fs', 'tp'), may hold values from -0.125 to 0.125
- in_scale: float32 [1, 1024], P(None, 'tp'), may hold values from 0.5 to 2
- pool_mix: bfloat16 [8, 128, 128], P('tp'), may hold values from -0.5 to 0.5
- pool_scale: float32 [1, 1024], P(None, 'tp'), may hold values from 0.1 to 1.9
- out_matrix: float32 [1024, 2048], P('tp', 'fs'), may hold values from -0.25 to 0.25
- out_scale: float32 [1, 2048], P(None, 'fs'), may hold values from 0.5 to 2
- ffn_gain: float32 [2048], replicated, may hold values from 0.1 to 1.9
- gate_matrix: float32 [2048, 5632], P('fs', 'tp'), may hold values from -0.125 to 0.125
- gate_scale: float32 [1, 5632], P(None, 'tp'), may hold values from 0.5 to 2
- up_matrix: float32 [2048, 5632], P('fs', 'tp'), may hold values from -0.125 to 0.125
- up_scale: float32 [1, 5632], P(None, 'tp'), may hold values from 0.5 to 2
- gate_taps: float32 [3, 5632], P(None, 'tp'), may hold values from -4 to 4
- up_taps: float32 [3, 5632], P(None, 'tp'), may hold values from -4 to 4
- down_matrix: float32 [5632, 2048], P('tp', 'fs'), may hold values from -0.109375 to 0.109375
- down_scale: float32 [1, 2048], P(None, 'fs'), may hold values from 0.5 to 2
Outputs:
- layer_out: bfloat16 [8, 1024, 2048], P(('grp', 'fs'), None, 'tp'), parts along dimension 0
There are 2 independent parts, one for each index of `grp`. A program takes and returns all parts, laid end to end along the dimension named above; an argument that names none is the same for every part. Nothing has to cross between parts.
All inputs are finite; a program needn't handle non-finite values.
Results may differ from a plain program's by a relative error of at most 0.025.
Values may be sent and summed in bfloat16 or wider, within the bound.
No kernel may reach another device: no remote copies, remote signals or barrier semaphores. Data moves between devices by JAX's collectives and lax.ppermute only.
A program may use at most 128 MiB of HBM per device.

v0:
```python
import jax
import jax.numpy as jnp
from jax import lax
from jax.sharding import PartitionSpec as P

BLOCKS = 8
eps = 1e-06
widest_span = 16


def norm_rows(tok_rows, norm_gain):
    values = tok_rows.astype(jnp.float32)
    scaled = values * lax.rsqrt(jnp.mean(values * values, axis=-1, keepdims=True) + eps)
    return (scaled * norm_gain).astype(jnp.bfloat16)


def span_widths(block_ids):
    return jnp.left_shift(jnp.ones_like(block_ids), 1 + 4 * block_ids // BLOCKS)


def trailing_gap(projected, windows):
    values = projected.astype(jnp.float32)
    length = values.shape[0]
    running = values
    for offset in range(1, widest_span):
        shifted = jnp.pad(values[: length - offset], ((offset, 0), (0, 0)))
        running = running + jnp.where(windows[None, :] > offset, shifted, jnp.zeros_like(shifted))
    positions = jnp.arange(length, dtype=jnp.int32)[:, None]
    counts = jnp.minimum(positions + 1, windows[None, :]).astype(jnp.float32)
    return (running / counts - values).astype(jnp.bfloat16)


def causal_taps(linear, tap_table):
    values = linear.astype(jnp.float32)
    length = values.shape[0]
    back_one = jnp.pad(values[: length - 1], ((1, 0), (0, 0)))
    back_two = jnp.pad(values[: length - 2], ((2, 0), (0, 0)))
    return tap_table[2] * values + tap_table[1] * back_one + tap_table[0] * back_two


def fold_rows(operand, portion):
    return jnp.dot(operand, portion, preferred_element_type=jnp.float32)


def shards(
    tokens,
    mix_gain,
    in_matrix,
    in_scale,
    pool_mix,
    pool_scale,
    out_matrix,
    out_scale,
    ffn_gain,
    gate_matrix,
    gate_scale,
    up_matrix,
    up_scale,
    gate_taps,
    up_taps,
    down_matrix,
    down_scale,
):
    length = tokens.shape[1]
    own_width = tokens.shape[2]
    local_rows = tokens.reshape(length, own_width)
    gathered = lax.all_gather(local_rows, "tp", axis=1, tiled=True)
    normed = norm_rows(gathered, mix_gain)
    width_in = in_matrix.shape[1]
    in_total = fold_rows(
        normed, lax.all_gather(in_matrix.astype(jnp.bfloat16), "fs", axis=0, tiled=True)
    )
    projected = (in_total * in_scale).astype(jnp.bfloat16)
    local_blocks = pool_mix.shape[0]
    block_width = pool_mix.shape[1]
    block_ids = lax.axis_index("tp") * local_blocks + jnp.arange(local_blocks, dtype=jnp.int32)
    windows = jnp.repeat(span_widths(block_ids), block_width)
    spread = trailing_gap(projected, windows)
    block_mixed = jnp.einsum(
        "lbc,bce->lbe",
        spread.reshape(length, local_blocks, block_width),
        pool_mix,
        preferred_element_type=jnp.float32,
    ).reshape(length, width_in)
    pooled = (block_mixed * pool_scale).astype(jnp.bfloat16)
    out_cols = lax.all_gather(out_scale, "fs", axis=1, tiled=True)
    tp_index = lax.axis_index("tp")
    groups = lax.axis_size("tp")
    pooled_all = lax.all_gather(pooled, "tp", axis=1, tiled=True)
    row_block = lax.all_gather(out_matrix.astype(jnp.bfloat16), "fs", axis=1, tiled=True)
    own_matrix = lax.all_to_all(row_block, "tp", split_axis=1, concat_axis=0, tiled=True)
    own_scales = lax.dynamic_slice_in_dim(out_cols, tp_index * own_width, own_width, 1)
    grouped_rows = pooled_all.reshape(length, groups, width_in)
    grouped_matrix = own_matrix.reshape(groups, width_in, own_width)
    pieces = (
        jnp.einsum("lgc,gcd->gld", grouped_rows, grouped_matrix, preferred_element_type=jnp.float32)
        * own_scales[None]
    )
    rounded = lax.optimization_barrier(pieces.astype(jnp.bfloat16))
    mixing = jnp.sum(rounded.astype(jnp.float32), axis=0)
    residual = (local_rows.astype(jnp.float32) + mixing).astype(jnp.bfloat16)
    gathered_ffn = lax.all_gather(residual, "tp", axis=1, tiled=True)
    normed_ffn = norm_rows(gathered_ffn, ffn_gain)
    gate_cast = gate_matrix.astype(jnp.bfloat16)
    up_cast = up_matrix.astype(jnp.bfloat16)
    gate_full, up_full = (
        lax.all_gather(gate_cast, "fs", axis=0, tiled=True),
        lax.all_gather(up_cast, "fs", axis=0, tiled=True),
    )
    gate_total = jnp.dot(normed_ffn, gate_full, preferred_element_type=jnp.float32)
    up_total = jnp.dot(normed_ffn, up_full, preferred_element_type=jnp.float32)
    gate_lin = (gate_total * gate_scale).astype(jnp.bfloat16)
    up_lin = (up_total * up_scale).astype(jnp.bfloat16)
    hidden = (jax.nn.silu(causal_taps(gate_lin, gate_taps)) * causal_taps(up_lin, up_taps)).astype(
        jnp.bfloat16
    )
    down_cols = lax.all_gather(down_scale, "fs", axis=1, tiled=True)
    partial_ffn = (
        jnp.dot(
            hidden,
            lax.all_gather(down_matrix.astype(jnp.bfloat16), "fs", axis=1, tiled=True),
            preferred_element_type=jnp.float32,
        )
        * down_cols
    )
    feed_out = lax.psum_scatter(
        partial_ffn.astype(jnp.bfloat16), "tp", scatter_dimension=1, tiled=True
    ).astype(jnp.float32)
    result = (residual.astype(jnp.float32) + feed_out).astype(jnp.bfloat16)
    return result.reshape(1, length, result.shape[1])


def solution(mesh):
    return jax.shard_map(
        shards,
        mesh=mesh,
        in_specs=(
            P(("grp", "fs"), None, "tp"),
            P(),
            P("fs", "tp"),
            P(None, "tp"),
            P("tp", None, None),
            P(None, "tp"),
            P("tp", "fs"),
            P(None, "fs"),
            P(),
            P("fs", "tp"),
            P(None, "tp"),
            P("fs", "tp"),
            P(None, "tp"),
            P(None, "tp"),
            P(None, "tp"),
            P("tp", "fs"),
            P(None, "fs"),
        ),
        out_specs=P(("grp", "fs"), None, "tp"),
        check_vma=False,
    )
```

profile of v0, /device:TPU:0, one launch (start us, length us, event | category | flops | bytes accessed | tf_op | source)
XLA Modules:
  0.0 573.4 jit_solution(17679194408588764987)
XLA Ops:
  6.5 0.7 all-gather.24.cloned.1.call-update
  7.3 1.8 convert_element_type.120
  9.1 0.0 all-gather.14.cloned.1.call-start
  9.2 1.9 copy.22
  11.1 0.0 all-gather.12.cloned.1.call-start
  11.1 0.1 bitcast_compare_fusion.14
  11.2 0.1 broadcast_bitcast_fusion
  11.3 34.8 %all-gather.24.cloned.1.call-done = bf16[1,1024,2048]{2,1,0:T(8,128)(2,1)} async-done(((bf16[1,1024,512]{2,1,0:T(8,128)(2,1)}), bf16[1,1024,2048]{2,1,0:T(8,128)(2,1)}) %all-gather.24.cloned.1.call-update) | async-done | bytes 4194320 | tf_op jit(solution)/shard_map/all_gather | solution.py:67
  46.1 3.1 fusion.3
  49.2 26.5 %all-gather.10.cloned.1.call-done = bf16[2048,256]{1,0:T(8,128)(2,1)} async-done(((bf16[512,256]{1,0:T(8,128)(2,1)}), bf16[2048,256]{1,0:T(8,128)(2,1)}) %all-gather.10.cloned.1.call-update) | async-done | bytes 1048592 | tf_op jit(solution)/shard_map/all_gather | solution.py:71
  75.7 3.8 fusion.20
  79.5 0.1 slice.107
  79.6 0.1 slice.108
  79.7 0.1 slice.109
  79.7 0.1 slice.110
  79.8 0.1 slice.111
  79.9 0.1 slice.112
  80.0 0.1 slice.113
  80.0 0.1 slice.114
  80.1 3.2 fusion.28
  83.4 0.9 fusion.26
  84.3 20.3 %all-gather.14.cloned.1.call-done = bf16[256,2048]{0,1:T(8,128)(2,1)} async-done(((bf16[256,512]{0,1:T(8,128)(2,1)}), bf16[256,2048]{0,1:T(8,128)(2,1)}) %all-gather.14.cloned.1.call-update) | async-done | bytes 1048592 | tf_op jit(solution)/shard_map/all_gather | solution.py:90
  104.7 2.3 copy.23
  106.9 3.5 all-to-all-start
  110.5 0.0 all-gather.16.cloned.1.call-start
  110.5 11.9 %all_gather.34 = f32[1,2048]{1,0:T(1,128)S(1)} all-gather(f32[1,512]{1,0:T(1,128)S(1)} %copy-done.10), channel_id=1, replica_groups=mesh['grp'=2,'fs'=4,'tp'=4] {'fs'}, dimensions={1}, use_global_device_ids=true | all-gather | bytes 10240 | tf_op jit(solution)/shard_map/all_gather | solution.py:86
  122.5 12.5 %all-to-all-done = bf16[256,4,512]{2,0,1:T(8,128)(2,1)S(1)} async-done(((bf16[256,4,512]{2,0,1:T(8,128)(2,1)}), bf16[256,4,512]{2,0,1:T(8,128)(2,1)S(1)}, u32[]{:S(2)}, u32[]{:S(2)}) %all-to-all-start) | async-done | bytes 1048608 | tf_op jit(solution)/shard_map/all_to_all | solution.py:91
  135.0 2.7 all-gather.12.cloned.1.call-done
  137.6 3.0 multiply_convert_fusion.1
  140.6 0.7 convert_reduce_fusion
  141.3 1.3 fusion.13
  142.7 0.0 all-gather.18.cloned.1.call-start
  142.7 1.3 convert_element_type.133
  144.1 0.0 all-gather.20.cloned.1.call-start
  144.2 3.3 convert_element_type.136
  147.5 1.3 convert_element_type.140
  149.0 12.1 %all_gather.39 = f32[1,2048]{1,0:T(1,128)S(1)} all-gather(f32[1,512]{1,0:T(1,128)S(1)} %copy-done.11), channel_id=1, replica_groups=mesh['grp'=2,'fs'=4,'tp'=4] {'fs'}, dimensions={1}, use_global_device_ids=true | all-gather | bytes 10240 | tf_op jit(solution)/shard_map/all_gather | solution.py:117
  161.1 0.1 slice_reduce_fusion.2
  161.2 14.5 %all-gather.16.cloned.1.call-done = bf16[1024,2048]{1,0:T(8,128)(2,1)} async-done(((bf16[1024,512]{1,0:T(8,128)(2,1)}), bf16[1024,2048]{1,0:T(8,128)(2,1)}) %all-gather.16.cloned.1.call-update) | async-done | bytes 4194320 | tf_op jit(solution)/shard_map/all_gather | solution.py:102
  175.7 3.1 fusion
  178.8 105.1 %all-gather.18.cloned.1.call-done = bf16[2048,1408]{1,0:T(8,128)(2,1)} async-done(((bf16[512,1408]{1,0:T(8,128)(2,1)}), bf16[2048,1408]{1,0:T(8,128)(2,1)}) %all-gather.18.cloned.1.call-update) | async-done | bytes 5767184 | tf_op jit(solution)/shard_map/all_gather | solution.py:107
  283.9 11.9 %fusion.11 = f32[1024,1408]{1,0:T(8,128)} fusion(bf16[2048,1408]{1,0:T(8,128)(2,1)} %all-gather.18.cloned.1.call-done, f32[1408]{0:T(1024)S(1)} %reduce.1, bf16[1024,2048]{1,0:T(8,128)(2,1)} %all-gather.16.cloned.1.call-done, f32[2048]{0:T(1024)S(1)} %copy-done.14, f32[1024]{0:T(1024)S(1)} %add_rsqrt_fusion), kind=kOutput, calls=%fused_computation.20 | convolution fusion | flops 5918294016 | bytes 15746560 | tf_op jit(solution)/shard_map/dot_general | solution.py:110
  295.8 94.7 %all-gather.20.cloned.1.call-done = bf16[2048,1408]{1,0:T(8,128)(2,1)} async-done(((bf16[512,1408]{1,0:T(8,128)(2,1)}), bf16[2048,1408]{1,0:T(8,128)(2,1)}) %all-gather.20.cloned.1.call-update) | async-done | bytes 5767184 | tf_op jit(solution)/shard_map/all_gather | solution.py:108
  390.4 12.0 %fusion.12 = f32[1024,1408]{1,0:T(8,128)} fusion(bf16[2048,1408]{1,0:T(8,128)(2,1)} %all-gather.20.cloned.1.call-done, f32[1408]{0:T(1024)S(1)} %reduce.5, bf16[1024,2048]{1,0:T(8,128)(2,1)} %all-gather.16.cloned.1.call-done, f32[2048]{0:T(1024)S(1)} %copy-done.14, f32[1024]{0:T(1024)S(1)} %add_rsqrt_fusion), kind=kOutput, calls=%fused_computation.21 | convolution fusion | flops 5918294016 | bytes 15746560 | tf_op jit(solution)/shard_map/dot_general | solution.py:111
  402.4 94.6 %all-gather.22.cloned.1.call-done = bf16[1408,2048]{1,0:T(8,128)(2,1)} async-done(((bf16[1408,512]{1,0:T(8,128)(2,1)}), bf16[1408,2048]{1,0:T(8,128)(2,1)}) %all-gather.22.cloned.1.call-update) | async-done | bytes 5767184 | tf_op jit(solution)/shard_map/all_gather | solution.py:121
  497.0 24.6 %multiply_convert_fusion = bf16[1024,2048]{1,0:T(8,128)(2,1)} fusion(bf16[1408,2048]{1,0:T(8,128)(2,1)} %all-gather.22.cloned.1.call-done, f32[2048]{0:T(1024)S(1)} %bitcast.83, f32[1022,1408]{1,0:T(8,128)} %bitcast.89, f32[1023,1408]{1,0:T(8,128)} %bitcast.90, f32[1024,1408]{1,0:T(8,128)} %fusion.12, f32[1022,1408]{1,0:T(8,128)} %bitcast.87, ...), kind=kOutput, calls=%fused_computation.10 | convolution fusion | flops 5932843008 | bytes 44572672 | tf_op jit(solution)/shard_map/dot_general | solution.py:119
  521.6 42.8 %reduce-scatter.2.cloned.1.call-done = bf16[1024,512]{1,0:T(8,128)(2,1)} async-done(((bf16[1024,2048]{1,0:T(8,128)(2,1)}), bf16[1024,512]{1,0:T(8,128)(2,1)}) %reduce-scatter.2.cloned.1.call-update) | async-done | bytes 1048592 | tf_op jit(solution)/shard_map/reduce_scatter | solution.py:126
  564.4 2.5 fusion.25
  (51 shorter events, 0.4 us)
Async XLA Ops:
  6.5 73.6 %copy-start = (bf16[2,128,128]{2,1,0:T(8,128)(2,1)S(1)}, bf16[2,128,128]{2,1,0:T(8,128)(2,1)}, u32[]{:S(2)}) copy-start(bf16[2,128,128]{2,1,0:T(8,128)(2,1)} %param.21) | copy-start | bytes 196612
  6.5 69.2 %copy-start.15 = (f32[1,256]{1,0:T(1,128)S(1)}, f32[1,256]{1,0:T(1,128)}, u32[]{:S(2)}) copy-start(f32[1,256]{1,0:T(1,128)} %param.20) | copy-start | bytes 3076
  6.5 69.2 %copy-start.13 = (f32[2048]{0:T(1024)S(1)}, f32[2048]{0:T(1024)}, u32[]{:S(2)}) copy-start(f32[2048]{0:T(1024)} %param.18) | copy-start | bytes 24580
  6.5 39.6 %all-gather.24.cloned.1.call-start = ((), (), s32[]{:S(2)}) async-start(), calls=%async_computation.10 | async-start | bytes 5242880 | tf_op jit(solution)/shard_map/all_gather | solution.py:67
  7.3 68.4 %all-gather.10.cloned.1.call-start = ((), (), s32[]{:S(2)}) async-start(), calls=%async_computation.2 | async-start | bytes 1310720 | tf_op jit(solution)/shard_map/all_gather | solution.py:71
  9.1 95.6 %all-gather.14.cloned.1.call-start = ((), (), s32[]{:S(2)}) async-start(), calls=%async_computation.4 | async-start | bytes 1310720 | tf_op jit(solution)/shard_map/all_gather | solution.py:90
  11.1 126.6 %all-gather.12.cloned.1.call-start = ((), (), s32[]{:S(2)}) async-start(), calls=%async_computation.3 | async-start | bytes 2621440 | tf_op jit(solution)/shard_map/all_gather | solution.py:89
  80.1 3.3 copy-start.12
  83.4 27.1 %copy-start.10 = (f32[1,512]{1,0:T(1,128)S(1)}, f32[1,512]{1,0:T(1,128)}, u32[]{:S(2)}) copy-start(f32[1,512]{1,0:T(1,128)} %param.24) | copy-start | bytes 6148
  106.9 28.0 %all-to-all-start = ((bf16[256,4,512]{2,0,1:T(8,128)(2,1)}), bf16[256,4,512]{2,0,1:T(8,128)(2,1)S(1)}, u32[]{:S(2)}, u32[]{:S(2)}) async-start(bf16[256,4,512]{2,0,1:T(8,128)(2,1)} %copy.23), calls=%async_computation | async-start | bytes 2097152 | tf_op jit(solution)/shard_map/all_to_all | solution.py:91
  110.5 65.3 %all-gather.16.cloned.1.call-start = ((), (), s32[]{:S(2)}) async-start(), calls=%async_computation.5 | async-start | bytes 5242880 | tf_op jit(solution)/shard_map/all_gather | solution.py:102
  137.6 3.7 copy-start.3
  140.6 2.1 copy-start.4
  142.7 141.2 %all-gather.18.cloned.1.call-start = ((), (), s32[]{:S(2)}) async-start(), calls=%async_computation.6 | async-start | bytes 7208960 | tf_op jit(solution)/shard_map/all_gather | solution.py:107
  144.0 3.5 copy-start.5
  144.1 4.8 copy-start.8
  144.1 4.9 copy-start.9
  144.1 4.9 copy-start.11
  144.1 17.0 %copy-start.6 = (f32[3,1408]{1,0:T(4,128)S(1)}, f32[3,1408]{1,0:T(4,128)}, u32[]{:S(2)}) copy-start(f32[3,1408]{1,0:T(4,128)} %param.31) | copy-start | bytes 50692
  144.1 17.0 %copy-start.7 = (f32[3,1408]{1,0:T(4,128)S(1)}, f32[3,1408]{1,0:T(4,128)}, u32[]{:S(2)}) copy-start(f32[3,1408]{1,0:T(4,128)} %param.30) | copy-start | bytes 50692
  144.1 246.3 %all-gather.20.cloned.1.call-start = ((), (), s32[]{:S(2)}) async-start(), calls=%async_computation.7 | async-start | bytes 7208960 | tf_op jit(solution)/shard_map/all_gather | solution.py:108
  147.5 136.4 %copy-start.14 = (f32[2048]{0:T(1024)S(1)}, f32[2048]{0:T(1024)}, u32[]{:S(2)}) copy-start(f32[2048]{0:T(1024)} %param.25) | copy-start | bytes 24580
  147.5 349.5 %all-gather.22.cloned.1.call-start = ((), (), s32[]{:S(2)}) async-start(), calls=%async_computation.8 | async-start | bytes 7208960 | tf_op jit(solution)/shard_map/all_gather | solution.py:121
  148.8 415.6 %reduce-scatter.2.cloned.1.call-start = ((), (), s32[]{:S(2)}) async-start(), calls=%async_computation.9 | async-start | bytes 5242880 | tf_op jit(solution)/shard_map/reduce_scatter | solution.py:126
  497.0 67.4 %copy-start.2 = (bf16[1024,512]{1,0:T(8,128)(2,1)S(1)}, bf16[1024,512]{1,0:T(8,128)(2,1)}, u32[]{:S(2)}) copy-start(bf16[1024,512]{1,0:T(8,128)(2,1)} %fusion.13) | copy-start | bytes 3145732
  497.0 69.9 %copy-start.1 = (bf16[2,128,128]{2,1,0:T(8,128)(2,1)S(1)}, bf16[2,128,128]{2,1,0:T(8,128)(2,1)}, u32[]{:S(2)}) copy-start(bf16[2,128,128]{2,1,0:T(8,128)(2,1)} %param.21) | copy-start | bytes 196612
Sparse Core Ops, SparseCore 0:
  8.9 37.1 all-gather.23
  47.7 27.9 all-gather.9
  77.3 27.3 all-gather.13
  106.1 31.4 all-gather.11
  142.8 32.9 all-gather.15
  177.2 106.6 all-gather.17
  285.5 104.9 all-gather.19
  392.0 104.9 all-gather.21
  521.8 42.6 reduce-scatter.1
where the time goes:
time: 574 us; the launch traced here: 573 us
  waiting for transfers between devices  449 us (78%)
  matrix products  58.5 us (10%)
  blocking collectives  24.1 us (4%)
  other arithmetic  19.3 us (3%)
  between operations  13.5 us (2%)
    all_gather x1, waiting for transfers between devices, shards(): lax.all_gather(gate_cast, 'fs', axis=0, tiled=True)  105 us
    all_gather x1, waiting for transfers between devices, shards(): lax.all_gather(up_cast, 'fs', axis=0, tiled=True)  94.7 us
    all_gather x1, waiting for transfers between devices, shards(): lax.all_gather(down_matrix.astype(jnp.bfloat16), 'fs', axis=1, tiled=True)  94.6 us
    reduce_scatter x1, waiting for transfers between devices, shards(): lax.psum_scatter(partial_ffn.astype(jnp.bfloat16), 'tp', scatter_dimensio...  42.8 us
    all_gather x1, waiting for transfers between devices, shards(): gathered = lax.all_gather(local_rows, 'tp', axis=1, tiled=True)  34.8 us
    all_gather x1, waiting for transfers between devices, shards(): lax.all_gather(in_matrix.astype(jnp.bfloat16), 'fs', axis=0, tiled=True)  26.5 us
    dot_general x1, matrix products, shards(): jnp.dot(hidden, lax.all_gather(down_matrix.astype(jnp.bfloat16), 'fs', ax...  24.6 us
    all_gather x1, waiting for transfers between devices, shards(): lax.all_gather(out_matrix.astype(jnp.bfloat16), 'fs', axis=1, tiled=True)  20.3 us
  transfers between devices with their start and end apart: 10, of which 10 were waited for; matrix products, arithmetic and copies ran while one was open for 9% of the time, Pallas kernels for 0%

commit v1 on v0

--- a/solution.py
+++ b/solution.py
@@ -6,6 +6,22 @@
 BLOCKS = 8
 eps = 1e-06
 widest_span = 16
+
+
+def _draw_forms(local_array):
+    n_dev_all = lax.axis_size("tp")
+    found = []
+    jj = 0
+    while jj < n_dev_all:
+        found.append((jj, (jj + 1) % n_dev_all))
+        jj += 1
+    current_arr = [None] * n_dev_all
+    current_arr[n_dev_all - 1] = local_array
+    for ii in range(n_dev_all - 2, -1, -1):
+        current_arr[ii] = lax.ppermute(current_arr[ii + 1], axis_name="tp", perm=found)
+    upper = jnp.concatenate(current_arr, axis=1)
+    w2 = (lax.axis_index("tp") + 1) * local_array.shape[1]
+    return jnp.roll(upper, w2, 1)
 
 
 def norm_rows(tok_rows, norm_gain):
@@ -64,7 +80,7 @@
     length = tokens.shape[1]
     own_width = tokens.shape[2]
     local_rows = tokens.reshape(length, own_width)
-    gathered = lax.all_gather(local_rows, "tp", axis=1, tiled=True)
+    gathered = _draw_forms(local_rows)
     normed = norm_rows(gathered, mix_gain)
     width_in = in_matrix.shape[1]
     in_total = fold_rows(

time: 574 us -> 539 us (0.939)
  waiting for transfers between devices: 449 us -> 407 us
  local copies, waits for them, and re-layouts: 4.94 us -> 11.8 us
    ppermute x0 -> x3, waiting for transfers between devices: none -> 39.2 us  [_draw_forms(): lax.ppermute(current_arr[ii + 1], axis_name='tp', perm=found)]
    all_gather x1 -> x0, waiting for transfers between devices: 34.8 us -> none  [shards(): gathered = lax.all_gather(local_rows, 'tp', axis=1, tiled=True)]
    all_gather x1, waiting for transfers between devices: 26.5 us -> 0.02 us  [shards(): lax.all_gather(in_matrix.astype(jnp.bfloat16), 'fs', axis=0, tiled=True)]
    all_gather x1, waiting for transfers between devices: 20.3 us -> 1.77 us  [shards(): lax.all_gather(out_matrix.astype(jnp.bfloat16), 'fs', axis=1, tiled=True)]
    unnamed x33 -> x40, local copies, waits for them, and re-layouts: 1.96 us -> 8.7 us
  transfers between devices with their start and end apart: 10 -> 12, of which waited for: 10 -> 11; matrix products, arithmetic and copies ran while one was open for 9% -> 10% of each run, Pallas kernels for 0% -> 0%
where the time goes in v1:
time: 539 us; the launch traced here: 538 us
  waiting for transfers between devices  407 us (76%)
  matrix products  58.5 us (11%)
  blocking collectives  24.1 us (4%)
  other arithmetic  19.2 us (4%)
  between operations  13.9 us (3%)
  local copies, waits for them, and re-layouts  11.8 us (2%)
    all_gather x1, waiting for transfers between devices, shards(): lax.all_gather(gate_cast, 'fs', axis=0, tiled=True)  105 us
    all_gather x1, waiting for transfers between devices, shards(): lax.all_gather(down_matrix.astype(jnp.bfloat16), 'fs', axis=1, tiled=True)  94.6 us
    all_gather x1, waiting for transfers between devices, shards(): lax.all_gather(up_cast, 'fs', axis=0, tiled=True)  94.5 us
    reduce_scatter x1, waiting for transfers between devices, shards(): lax.psum_scatter(partial_ffn.astype(jnp.bfloat16), 'tp', scatter_dimensio...  42.8 us
    ppermute x3, waiting for transfers between devices, _draw_forms(): lax.ppermute(current_arr[ii + 1], axis_name='tp', perm=found)  39.2 us
    dot_general x1, matrix products, shards(): jnp.dot(hidden, lax.all_gather(down_matrix.astype(jnp.bfloat16), 'fs', ax...  24.6 us
    all_gather x1, waiting for transfers between devices, shards(): gathered_ffn = lax.all_gather(residual, 'tp', axis=1, tiled=True)  13.4 us
    all_to_all x1, waiting for transfers between devices, shards(): lax.all_to_all(row_block, 'tp', split_axis=1, concat_axis=0, tiled=True)  12.3 us
  transfers between devices with their start and end apart: 12, of which 11 were waited for; matrix products, arithmetic and copies ran while one was open for 10% of the time, Pallas kernels for 0%

profile of v1, /device:TPU:0, one launch (start us, length us, event | category | flops | bytes accessed | tf_op | source)
XLA Modules:
  0.0 538.3 jit_solution(614038206354753600)
XLA Ops:
  6.5 0.5 collective-permute-start
  7.0 1.8 convert_element_type.120
  8.9 12.8 %collective-permute-done = bf16[1024,512]{1,0:T(8,128)(2,1)S(1)} collective-permute-done((bf16[1024,512]{1,0:T(8,128)(2,1)}, bf16[1024,512]{1,0:T(8,128)(2,1)S(1)}, u32[]{:S(2)}, u32[]{:S(2)}) %collective-permute-start) | collective-permute-done | bytes 1048608 | tf_op jit(solution)/shard_map/ppermute | solution.py:21
  21.7 14.2 %collective-permute-done.1 = bf16[1024,512]{1,0:T(8,128)(2,1)S(1)} collective-permute-done((bf16[1024,512]{1,0:T(8,128)(2,1)S(1)}, bf16[1024,512]{1,0:T(8,128)(2,1)S(1)}, u32[]{:S(2)}, u32[]{:S(2)}) %collective-permute-start.1) | collective-permute-done | bytes 1048608 | tf_op jit(solution)/shard_map/ppermute | solution.py:21
  35.9 1.9 copy.22
  37.9 0.1 broadcast_bitcast_fusion
  38.0 0.1 bitcast_compare_fusion.14
  38.1 12.2 %collective-permute-done.2 = bf16[1024,512]{1,0:T(8,128)(2,1)} collective-permute-done((bf16[1024,512]{1,0:T(8,128)(2,1)S(1)}, bf16[1024,512]{1,0:T(8,128)(2,1)}, u32[]{:S(2)}, u32[]{:S(2)}) %collective-permute-start.2) | collective-permute-done | bytes 1048608 | tf_op jit(solution)/shard_map/ppermute | solution.py:21
  50.2 1.4 constant_dynamic-update-slice_fusion.7
  51.6 0.2 constant_dynamic-update-slice_fusion.6
  51.8 0.2 constant_dynamic-update-slice_fusion.5
  51.9 0.1 constant_dynamic-update-slice_fusion.4
  52.1 1.4 constant_dynamic-update-slice_fusion.3
  53.5 0.1 constant_dynamic-update-slice_fusion.2
  53.7 0.2 constant_dynamic-update-slice_fusion.1
  53.8 0.2 constant_dynamic-update-slice_fusion
  54.0 3.2 copy-done.4
  57.2 0.9 fusion
  58.2 3.8 fusion.19
  62.2 0.1 slice.109
  62.2 0.1 slice.110
  62.3 0.1 slice.111
  62.6 3.2 fusion.27
  65.9 0.9 fusion.25
  66.8 1.8 all-gather.12.cloned.1.call-done
  68.6 2.3 copy.23
  70.9 3.5 all-to-all-start
  74.5 11.9 %all_gather.30 = f32[1,2048]{1,0:T(1,128)S(1)} all-gather(f32[1,512]{1,0:T(1,128)S(1)} %copy-done.10), channel_id=1, replica_groups=mesh['grp'=2,'fs'=4,'tp'=4] {'fs'}, dimensions={1}, use_global_device_ids=true | all-gather | bytes 10240 | tf_op jit(solution)/shard_map/all_gather | solution.py:102
  86.4 12.3 %all-to-all-done = bf16[256,4,512]{2,0,1:T(8,128)(2,1)S(1)} async-done(((bf16[256,4,512]{2,0,1:T(8,128)(2,1)}), bf16[256,4,512]{2,0,1:T(8,128)(2,1)S(1)}, u32[]{:S(2)}, u32[]{:S(2)}) %all-to-all-start) | async-done | bytes 1048608 | tf_op jit(solution)/shard_map/all_to_all | solution.py:107
  98.7 2.8 all-gather.10.cloned.1.call-done
  101.6 2.9 multiply_convert_fusion.1
  104.5 0.7 convert_reduce_fusion
  105.1 1.3 add_convert_fusion.1
  106.5 3.3 convert_element_type.133
  109.9 1.3 convert_element_type.136
  111.3 3.4 convert_element_type.140
  114.9 12.1 %all_gather.35 = f32[1,2048]{1,0:T(1,128)S(1)} all-gather(f32[1,512]{1,0:T(1,128)S(1)} %copy-done.11), channel_id=1, replica_groups=mesh['grp'=2,'fs'=4,'tp'=4] {'fs'}, dimensions={1}, use_global_device_ids=true | all-gather | bytes 10240 | tf_op jit(solution)/shard_map/all_gather | solution.py:133
  127.0 0.1 slice_reduce_fusion.2
  127.1 13.4 %all-gather.14.cloned.1.call-done = bf16[1024,2048]{1,0:T(8,128)(2,1)} async-done(((bf16[1024,512]{1,0:T(8,128)(2,1)}), bf16[1024,2048]{1,0:T(8,128)(2,1)}) %all-gather.14.cloned.1.call-update) | async-done | bytes 4194320 | tf_op jit(solution)/shard_map/all_gather | solution.py:118
  140.4 3.1 fusion.3
  143.5 105.1 %all-gather.16.cloned.1.call-done = bf16[2048,1408]{1,0:T(8,128)(2,1)} async-done(((bf16[512,1408]{1,0:T(8,128)(2,1)}), bf16[2048,1408]{1,0:T(8,128)(2,1)}) %all-gather.16.cloned.1.call-update) | async-done | bytes 5767184 | tf_op jit(solution)/shard_map/all_gather | solution.py:123
  248.6 11.9 %fusion.10 = f32[1024,1408]{1,0:T(8,128)} fusion(bf16[2048,1408]{1,0:T(8,128)(2,1)} %all-gather.16.cloned.1.call-done, f32[1408]{0:T(1024)S(1)} %reduce.1, bf16[1024,2048]{1,0:T(8,128)(2,1)} %all-gather.14.cloned.1.call-done, f32[2048]{0:T(1024)S(1)} %copy-done.14, f32[1024]{0:T(1024)S(1)} %add_rsqrt_fusion), kind=kOutput, calls=%fused_computation.19 | convolution fusion | flops 5918294016 | bytes 15746560 | tf_op jit(solution)/shard_map/dot_general | solution.py:126
  260.5 94.5 %all-gather.18.cloned.1.call-done = bf16[2048,1408]{1,0:T(8,128)(2,1)} async-done(((bf16[512,1408]{1,0:T(8,128)(2,1)}), bf16[2048,1408]{1,0:T(8,128)(2,1)}) %all-gather.18.cloned.1.call-update) | async-done | bytes 5767184 | tf_op jit(solution)/shard_map/all_gather | solution.py:124
  355.0 12.0 %fusion.11 = f32[1024,1408]{1,0:T(8,128)} fusion(bf16[2048,1408]{1,0:T(8,128)(2,1)} %all-gather.18.cloned.1.call-done, f32[1408]{0:T(1024)S(1)} %reduce.5, bf16[1024,2048]{1,0:T(8,128)(2,1)} %all-gather.14.cloned.1.call-done, f32[2048]{0:T(1024)S(1)} %copy-done.14, f32[1024]{0:T(1024)S(1)} %add_rsqrt_fusion), kind=kOutput, calls=%fused_computation.20 | convolution fusion | flops 5918294016 | bytes 15746560 | tf_op jit(solution)/shard_map/dot_general | solution.py:127
  367.0 94.6 %all-gather.20.cloned.1.call-done = bf16[1408,2048]{1,0:T(8,128)(2,1)} async-done(((bf16[1408,512]{1,0:T(8,128)(2,1)}), bf16[1408,2048]{1,0:T(8,128)(2,1)}) %all-gather.20.cloned.1.call-update) | async-done | bytes 5767184 | tf_op jit(solution)/shard_map/all_gather | solution.py:137
  461.5 24.6 %multiply_convert_fusion = bf16[1024,2048]{1,0:T(8,128)(2,1)} fusion(bf16[1408,2048]{1,0:T(8,128)(2,1)} %all-gather.20.cloned.1.call-done, f32[2048]{0:T(1024)S(1)} %bitcast.72, f32[1022,1408]{1,0:T(8,128)} %bitcast.78, f32[1023,1408]{1,0:T(8,128)} %bitcast.79, f32[1024,1408]{1,0:T(8,128)} %fusion.11, f32[1022,1408]{1,0:T(8,128)} %bitcast.76, ...), kind=kOutput, calls=%fused_computation.10 | convolution fusion | flops 5932843008 | bytes 44572672 | tf_op jit(solution)/shard_map/dot_general | solution.py:135
  486.2 42.8 %reduce-scatter.2.cloned.1.call-done = bf16[1024,512]{1,0:T(8,128)(2,1)} async-done(((bf16[1024,2048]{1,0:T(8,128)(2,1)}), bf16[1024,512]{1,0:T(8,128)(2,1)}) %reduce-scatter.2.cloned.1.call-update) | async-done | bytes 1048592 | tf_op jit(solution)/shard_map/reduce_scatter | solution.py:142
  529.0 2.5 fusion.24
  (62 shorter events, 1.0 us)
Async XLA Ops:
  6.5 56.1 %copy-start = (bf16[2,128,128]{2,1,0:T(8,128)(2,1)S(1)}, bf16[2,128,128]{2,1,0:T(8,128)(2,1)}, u32[]{:S(2)}) copy-start(bf16[2,128,128]{2,1,0:T(8,128)(2,1)} %param.21) | copy-start | bytes 196612
  6.5 45.4 %copy-start.3 = (bf16[1,1024,512]{2,1,0:T(8,128)(2,1)S(1)}, bf16[1,1024,512]{2,1,0:T(8,128)(2,1)}, u32[]{:S(2)}) copy-start(bf16[1,1024,512]{2,1,0:T(8,128)(2,1)} %param.17) | copy-start | bytes 3145732
  6.5 51.6 %all-gather.8.cloned.1.call-start = ((), (), s32[]{:S(2)}) async-start(), calls=%async_computation.2 | async-start | bytes 1310720 | tf_op jit(solution)/shard_map/all_gather | solution.py:87
  6.5 15.1 %collective-permute-start = (bf16[1024,512]{1,0:T(8,128)(2,1)}, bf16[1024,512]{1,0:T(8,128)(2,1)S(1)}, u32[]{:S(2)}, u32[]{:S(2)}) collective-permute-start(bf16[1024,512]{1,0:T(8,128)(2,1)} %bitcast.69), channel_id=1, source_target_pairs={{0,1},{1,2},{2,3},{3,0},{4,5},{5,6},{6,7},{7,4},{8,9},{9,10},{10,1... | collective-permute-start | bytes 3145736 | tf_op jit(solution)/shard_map/ppermute | solution.py:21
  8.8 59.8 %all-gather.12.cloned.1.call-start = ((), (), s32[]{:S(2)}) async-start(), calls=%async_computation.4 | async-start | bytes 1310720 | tf_op jit(solution)/shard_map/all_gather | solution.py:106
  21.7 14.2 %collective-permute-start.1 = (bf16[1024,512]{1,0:T(8,128)(2,1)S(1)}, bf16[1024,512]{1,0:T(8,128)(2,1)S(1)}, u32[]{:S(2)}, u32[]{:S(2)}) collective-permute-start(bf16[1024,512]{1,0:T(8,128)(2,1)S(1)} %collective-permute-done), channel_id=1, source_target_pairs={{0,1},{1,2},{2,3},{3,0},{4,5},{5,6},{6,7},{7,4},{8,9},{9,10},{10,1... | collective-permute-start | bytes 3145736 | tf_op jit(solution)/shard_map/ppermute | solution.py:21
  35.9 14.3 %collective-permute-start.2 = (bf16[1024,512]{1,0:T(8,128)(2,1)S(1)}, bf16[1024,512]{1,0:T(8,128)(2,1)}, u32[]{:S(2)}, u32[]{:S(2)}) collective-permute-start(bf16[1024,512]{1,0:T(8,128)(2,1)S(1)} %collective-permute-done.1), channel_id=1, source_target_pairs={{0,1},{1,2},{2,3},{3,0},{4,5},{5,6},{6,7},{7,4},{8,9},{9,10},{10,1... | collective-permute-start | bytes 3145736 | tf_op jit(solution)/shard_map/ppermute | solution.py:21
  37.8 63.7 %all-gather.10.cloned.1.call-start = ((), (), s32[]{:S(2)}) async-start(), calls=%async_computation.3 | async-start | bytes 2621440 | tf_op jit(solution)/shard_map/all_gather | solution.py:105
  53.5 4.7 copy-start.13
  53.5 4.7 copy-start.15
  54.0 3.2 copy-start.4
  62.6 3.2 copy-start.12
  65.9 8.6 %copy-start.10 = (f32[1,512]{1,0:T(1,128)S(1)}, f32[1,512]{1,0:T(1,128)}, u32[]{:S(2)}) copy-start(f32[1,512]{1,0:T(1,128)} %param.24) | copy-start | bytes 6148
  70.9 27.9 %all-to-all-start = ((bf16[256,4,512]{2,0,1:T(8,128)(2,1)}), bf16[256,4,512]{2,0,1:T(8,128)(2,1)S(1)}, u32[]{:S(2)}, u32[]{:S(2)}) async-start(bf16[256,4,512]{2,0,1:T(8,128)(2,1)} %copy.23), calls=%async_computation | async-start | bytes 2097152 | tf_op jit(solution)/shard_map/all_to_all | solution.py:107
  74.4 66.0 %all-gather.14.cloned.1.call-start = ((), (), s32[]{:S(2)}) async-start(), calls=%async_computation.5 | async-start | bytes 5242880 | tf_op jit(solution)/shard_map/all_gather | solution.py:118
  106.4 3.5 copy-start.5
  106.5 142.1 %all-gather.16.cloned.1.call-start = ((), (), s32[]{:S(2)}) async-start(), calls=%async_computation.6 | async-start | bytes 7208960 | tf_op jit(solution)/shard_map/all_gather | solution.py:123
  109.8 5.0 copy-start.8
  109.8 5.0 copy-start.9
  109.8 5.0 copy-start.11
  109.9 17.1 %copy-start.6 = (f32[3,1408]{1,0:T(4,128)S(1)}, f32[3,1408]{1,0:T(4,128)}, u32[]{:S(2)}) copy-start(f32[3,1408]{1,0:T(4,128)} %param.31) | copy-start | bytes 50692
  109.9 17.1 %copy-start.7 = (f32[3,1408]{1,0:T(4,128)S(1)}, f32[3,1408]{1,0:T(4,128)}, u32[]{:S(2)}) copy-start(f32[3,1408]{1,0:T(4,128)} %param.30) | copy-start | bytes 50692
  109.9 245.1 %all-gather.18.cloned.1.call-start = ((), (), s32[]{:S(2)}) async-start(), calls=%async_computation.7 | async-start | bytes 7208960 | tf_op jit(solution)/shard_map/all_gather | solution.py:124
  111.3 137.3 %copy-start.14 = (f32[2048]{0:T(1024)S(1)}, f32[2048]{0:T(1024)}, u32[]{:S(2)}) copy-start(f32[2048]{0:T(1024)} %param.25) | copy-start | bytes 24580
  111.3 350.2 %all-gather.20.cloned.1.call-start = ((), (), s32[]{:S(2)}) async-start(), calls=%async_computation.8 | async-start | bytes 7208960 | tf_op jit(solution)/shard_map/all_gather | solution.py:137
  114.7 414.3 %reduce-scatter.2.cloned.1.call-start = ((), (), s32[]{:S(2)}) async-start(), calls=%async_computation.9 | async-start | bytes 5242880 | tf_op jit(solution)/shard_map/reduce_scatter | solution.py:142
  461.5 67.5 %copy-start.2 = (bf16[1024,512]{1,0:T(8,128)(2,1)S(1)}, bf16[1024,512]{1,0:T(8,128)(2,1)}, u32[]{:S(2)}) copy-start(bf16[1024,512]{1,0:T(8,128)(2,1)} %add_convert_fusion.1) | copy-start | bytes 3145732
  461.5 70.0 %copy-start.1 = (bf16[2,128,128]{2,1,0:T(8,128)(2,1)S(1)}, bf16[2,128,128]{2,1,0:T(8,128)(2,1)}, u32[]{:S(2)}) copy-start(bf16[2,128,128]{2,1,0:T(8,128)(2,1)} %param.21) | copy-start | bytes 196612
Sparse Core Ops, SparseCore 0:
  8.9 30.6 all-gather.7
  41.2 27.3 all-gather.11
  70.2 31.3 all-gather.9
  106.6 33.8 all-gather.13
  141.9 106.6 all-gather.15
  250.0 104.9 all-gather.17
  356.5 104.9 all-gather.19
  486.3 42.6 reduce-scatter.1
